TPU v7x, 32 devices: a whole 2x2x4 slice. The times are simulated.
32 devices in a mesh: grp: 2 (over x), fs: 4 (over z), tp: 4 (over y, core).
Axes of the slice: x: 2, y: 2, z: 4, core: 2. Of those that a mesh axis runs over, the one named last changes fastest.
Arguments:
- stream: bfloat16 [2048, 2048], P(('grp', 'fs'), 'tp'), parts along dimension 0, may hold values from -80 to 80
- mixed: bfloat16 [2048, 2048], P(('grp', 'fs'), 'tp'), parts along dimension 0, may hold values from -6 to 6
- out_weight: bfloat16 [2048, 2048], P('fs', 'tp'), may hold values from -0.125 to 0.125
- norm_gain: bfloat16 [2048], P('tp'), may hold values from 0.099609375 to 1.8984375
- up_weight: bfloat16 [2048, 8192], P('fs', 'tp'), may hold values from -0.125 to 0.125
- down_weight: bfloat16 [8192, 2048], P('tp', 'fs'), may hold values from -0.09375 to 0.09375
Outputs:
- result: bfloat16 [2048, 2048], P(('grp', 'fs'), 'tp'), parts along dimension 0
There are 2 independent parts, one for each index of `grp`. A program takes and returns all parts, laid end to end along the dimension named above; an argument that names none is the same for every part. Nothing has to cross between parts.
All inputs are finite; a program needn't handle non-finite values.
Results may differ from a plain program's by a relative error of at most 0.01.
Values may be sent and summed in bfloat16 or wider, within the bound.
A program may use at most 64 MiB of HBM per device.

v0:
```python
import jax
import jax.numpy as jnp
from jax import lax
from jax.sharding import PartitionSpec as P

epsilon = 1e-06


def fold_product(left, portion):
    return jnp.dot(left, portion, preferred_element_type=jnp.float32)


def gathered_body(stream, mixed, out_weight, norm_gain, up_weight, down_weight):
    mixed_whole = lax.all_gather(mixed, "tp", axis=1, tiled=True)
    projected = fold_product(mixed_whole, lax.all_gather(out_weight, "fs", axis=0, tiled=True))
    resid = (stream.astype(jnp.float32) + projected).astype(jnp.bfloat16)
    widened = resid.astype(jnp.float32)
    resid_whole, gain_whole = (
        lax.all_gather(resid, "tp", axis=1, tiled=True),
        lax.all_gather(norm_gain, "tp", axis=0, tiled=True),
    )
    stream_wide = resid_whole.astype(jnp.float32)
    energy = jnp.mean(stream_wide * stream_wide, axis=1, keepdims=True)
    normed_whole = (
        stream_wide * lax.rsqrt(energy + epsilon) * gain_whole.astype(jnp.float32)
    ).astype(jnp.bfloat16)
    up_full = lax.all_gather(up_weight, "fs", axis=0, tiled=True)
    up_values = jnp.dot(normed_whole, up_full, preferred_element_type=jnp.float32)
    activated = jnp.square(jax.nn.relu(up_values)).astype(jnp.bfloat16)
    partials = jnp.dot(
        activated,
        lax.all_gather(down_weight, "fs", axis=1, tiled=True),
        preferred_element_type=jnp.float32,
    )
    branch = lax.psum_scatter(partials, "tp", scatter_dimension=1, tiled=True)
    return (widened + branch).astype(jnp.bfloat16)


def spread_body(stream, mixed, out_weight, norm_gain, up_weight, down_weight):
    mixed_whole = lax.all_gather(mixed, "tp", axis=1, tiled=True)
    out_full = lax.all_gather(out_weight, "fs", axis=0, tiled=True)
    up_mine = lax.all_to_all(up_weight, "fs", split_axis=1, concat_axis=0, tiled=True)
    down_mine = lax.all_to_all(down_weight, "fs", split_axis=0, concat_axis=1, tiled=True)
    projected = jnp.dot(mixed_whole, out_full, preferred_element_type=jnp.float32)
    resid = (stream.astype(jnp.float32) + projected).astype(jnp.bfloat16)
    rows = lax.all_gather(resid, "fs", axis=0, tiled=True)
    whole = lax.all_gather(rows, "tp", axis=1, tiled=True).astype(jnp.float32)
    gain = lax.all_gather(norm_gain, "tp", axis=0, tiled=True).astype(jnp.float32)
    energy = jnp.mean(whole * whole, axis=1, keepdims=True)
    normed = (whole * lax.rsqrt(energy + epsilon) * gain).astype(jnp.bfloat16)
    up_values = jnp.dot(normed, up_mine, preferred_element_type=jnp.float32)
    activated = jnp.square(jax.nn.relu(up_values)).astype(jnp.bfloat16)
    partials = jnp.dot(activated, down_mine, preferred_element_type=jnp.float32).astype(
        jnp.bfloat16
    )
    columns = lax.psum_scatter(partials, "tp", scatter_dimension=1, tiled=True)
    branch = lax.psum_scatter(columns, "fs", scatter_dimension=0, tiled=True)
    return (resid.astype(jnp.float32) + branch.astype(jnp.float32)).astype(jnp.bfloat16)


def solution(mesh):
    placed = (
        P(("grp", "fs"), "tp"),
        P(("grp", "fs"), "tp"),
        P("fs", "tp"),
        P("tp"),
        P("fs", "tp"),
        P("tp", "fs"),
    )
    fs, tp = (mesh.shape["fs"], mesh.shape["tp"])

    def call(stream, mixed, out_weight, norm_gain, up_weight, down_weight):
        width, hidden = up_weight.shape
        tokens = stream.shape[0] // mesh.shape["grp"]
        moved_weights = 2 * width * hidden // tp
        moved_rows = 2 * tokens * width + 2 * width * hidden // (tp * fs)
        body = spread_body if moved_rows < moved_weights else gathered_body
        return sharded(body)(stream, mixed, out_weight, norm_gain, up_weight, down_weight)

    def sharded(body):
        return jax.shard_map(
            body, mesh=mesh, in_specs=placed, out_specs=P(("grp", "fs"), "tp"), check_vma=False
        )

    return call
```

profile of v0, /device:TPU:0, one launch (start us, length us, event | category | flops | bytes accessed | tf_op | source)
XLA Modules:
  0.0 298.6 jit_solution(17435808376531385950)
XLA Ops:
  6.5 0.7 all-gather.6.cloned.1.call-update
  7.3 0.0 all-gather.8.cloned.1.call-start
  7.3 0.7 all-gather.8.cloned.1.call-update
  8.0 0.0 all-gather.10.cloned.1.call-start
  8.1 20.3 %all-gather.6.cloned.1.call-done = bf16[256,2048]{1,0:T(8,128)(2,1)} async-done(((bf16[256,512]{1,0:T(8,128)(2,1)}), bf16[256,2048]{1,0:T(8,128)(2,1)}) %all-gather.6.cloned.1.call-update) | async-done | bytes 1048592 | tf_op jit(solution)/shard_map/all_gather | solution.py:40
  28.4 47.3 %all-gather.8.cloned.1.call-done = bf16[2048,512]{1,0:T(8,128)(2,1)} async-done(((bf16[512,512]{1,0:T(8,128)(2,1)}), bf16[2048,512]{1,0:T(8,128)(2,1)}) %all-gather.8.cloned.1.call-update) | async-done | bytes 2097168 | tf_op jit(solution)/shard_map/all_gather | solution.py:41
  75.6 3.3 %fusion.9 = bf16[256,512]{1,0:T(8,128)(2,1)} fusion(bf16[256,2048]{1,0:T(8,128)(2,1)} %all-gather.6.cloned.1.call-done, bf16[2048,512]{1,0:T(8,128)(2,1)} %all-gather.8.cloned.1.call-done, bf16[256,512]{1,0:T(8,128)(2,1)} %param.6), kind=kOutput, calls=%fused_computation.11 | convolution fusion | flops 537264128 | bytes 3670016 | tf_op jit(solution)/shard_map/dot_general | solution.py:44
  78.9 3.6 %all-to-all-start.1 = ((bf16[4,512,512]{2,1,0:T(8,128)(2,1)}), bf16[4,512,512]{2,1,0:T(8,128)(2,1)S(1)}, u32[]{:S(2)}, u32[]{:S(2)}) async-start(bf16[4,512,512]{2,1,0:T(8,128)(2,1)} %bitcast.13), calls=%async_computation.1 | async-start | bytes 4194304 | tf_op jit(solution)/shard_map/all_to_all | solution.py:43
  82.6 0.0 all-gather.12.cloned.1.call-start
  82.6 41.1 %all-gather.10.cloned.1.call-done = bf16[1024,512]{1,0:T(8,128)(2,1)} async-done(((bf16[256,512]{1,0:T(8,128)(2,1)}), bf16[1024,512]{1,0:T(8,128)(2,1)}) %all-gather.10.cloned.1.call-update) | async-done | bytes 1048592 | tf_op jit(solution)/shard_map/all_gather | solution.py:46
  123.8 4.0 %copy.10 = bf16[512,2048]{0,1:T(8,128)(2,1)} copy(bf16[512,2048]{1,0:T(8,128)(2,1)} %param.10) | data formatting | bytes 4194304 | tf_op args[4]
  127.7 20.0 %all-to-all-done.1 = bf16[4,512,512]{2,1,0:T(8,128)(2,1)S(1)} async-done(((bf16[4,512,512]{2,1,0:T(8,128)(2,1)}), bf16[4,512,512]{2,1,0:T(8,128)(2,1)S(1)}, u32[]{:S(2)}, u32[]{:S(2)}) %all-to-all-start.1) | async-done | bytes 2097184 | tf_op jit(solution)/shard_map/all_to_all | solution.py:43
  147.7 4.6 %all-to-all-start = ((bf16[512,4,512]{0,2,1:T(8,128)(2,1)}), bf16[512,4,512]{0,2,1:T(8,128)(2,1)}, u32[]{:S(2)}, u32[]{:S(2)}) async-start(bf16[512,4,512]{0,2,1:T(8,128)(2,1)} %bitcast.12), calls=%async_computation | async-start | bytes 4194304 | tf_op jit(solution)/shard_map/all_to_all | solution.py:42
  152.3 0.0 reduce-scatter.3.cloned.1.call-start
  152.4 5.4 %all-gather = bf16[4,1,512]{2,1,0:T(2,128)(2,1)S(1)} all-gather(bf16[1,1,512]{2,1,0:T(2,128)(2,1)S(1)} %reshape.15), channel_id=1, replica_groups=mesh['grp'=2,'fs'=4,'tp'=4] {'tp'}, dimensions={0}, use_global_device_ids=true | all-gather | bytes 5120 | tf_op jit(solution)/shard_map/all_gather | solution.py:48
  157.7 2.4 copy.12
  160.1 40.0 %all-to-all-done = bf16[512,4,512]{0,2,1:T(8,128)(2,1)} async-done(((bf16[512,4,512]{0,2,1:T(8,128)(2,1)}), bf16[512,4,512]{0,2,1:T(8,128)(2,1)}, u32[]{:S(2)}, u32[]{:S(2)}) %all-to-all-start) | async-done | bytes 2097184 | tf_op jit(solution)/shard_map/all_to_all | solution.py:42
  200.1 4.2 %copy.11 = bf16[4,512,512]{2,1,0:T(8,128)(2,1)} copy(bf16[4,512,512]{1,2,0:T(8,128)(2,1)} %bitcast.2) | data formatting | bytes 4194304 | tf_op jit(solution)/shard_map/all_to_all | solution.py:42
  204.3 3.2 %fusion = f32[1024]{0:T(1024)S(1)} fusion(bf16[1024,2048]{1,0:T(8,128)(2,1)} %all-gather.12.cloned.1.call-done), kind=kLoop, calls=%fused_computation.2 | loop fusion | flops 6290432 | bytes 4198400 | tf_op jit(solution)/shard_map/reduce_sum | solution.py:49
  207.6 9.4 %convolution_convert_fusion = bf16[1024,2048]{1,0:T(8,128)(2,1)} fusion(bf16[512,2048]{0,1:T(8,128)(2,1)S(1)} %bitcast.14, bf16[2048,512]{1,0:T(8,128)(2,1)} %bitcast.15, bf16[1024,2048]{1,0:T(8,128)(2,1)} %all-gather.12.cloned.1.call-done, f32[2048]{0:T(1024)S(1)} %bitcast.16, f32[1024]{0:T(1024)S(1)} %add_rsqrt_fusion), kind=kOutput, calls=%fused_computation.8 | convolution fusion | flops 4307025920 | bytes 12595200 | tf_op jit(solution)/shard_map/dot_general | solution.py:53
  217.0 0.0 reduce-scatter.5.cloned.1.call-start
  217.0 43.6 %reduce-scatter.3.cloned.1.call-done = bf16[1024,512]{1,0:T(8,128)(2,1)} async-done(((bf16[1024,2048]{1,0:T(8,128)(2,1)}), bf16[1024,512]{1,0:T(8,128)(2,1)}) %reduce-scatter.3.cloned.1.call-update) | async-done | bytes 1048592 | tf_op jit(solution)/shard_map/reduce_scatter | solution.py:56
  260.6 29.4 %reduce-scatter.5.cloned.1.call-done = bf16[256,512]{1,0:T(8,128)(2,1)} async-done(((bf16[1024,512]{1,0:T(8,128)(2,1)}), bf16[256,512]{1,0:T(8,128)(2,1)}) %reduce-scatter.5.cloned.1.call-update) | async-done | bytes 262160 | tf_op jit(solution)/shard_map/reduce_scatter | solution.py:57
  290.1 1.7 add_convert_fusion
  (15 shorter events, 0.1 us)
Async XLA Ops:
  6.5 21.8 %all-gather.6.cloned.1.call-start = ((), (), s32[]{:S(2)}) async-start(), calls=%async_computation.4 | async-start | bytes 1310720 | tf_op jit(solution)/shard_map/all_gather | solution.py:40
  7.3 68.3 %all-gather.8.cloned.1.call-start = ((), (), s32[]{:S(2)}) async-start(), calls=%async_computation.5 | async-start | bytes 2621440 | tf_op jit(solution)/shard_map/all_gather | solution.py:41
  8.0 115.8 %all-gather.10.cloned.1.call-start = ((), (), s32[]{:S(2)}) async-start(), calls=%async_computation.6 | async-start | bytes 1310720 | tf_op jit(solution)/shard_map/all_gather | solution.py:46
  78.9 68.8 %all-to-all-start.1 = ((bf16[4,512,512]{2,1,0:T(8,128)(2,1)}), bf16[4,512,512]{2,1,0:T(8,128)(2,1)S(1)}, u32[]{:S(2)}, u32[]{:S(2)}) async-start(bf16[4,512,512]{2,1,0:T(8,128)(2,1)} %bitcast.13), calls=%async_computation.1 | async-start | bytes 4194304 | tf_op jit(solution)/shard_map/all_to_all | solution.py:43
  82.6 121.7 %all-gather.12.cloned.1.call-start = ((), (), s32[]{:S(2)}) async-start(), calls=%async_computation.7 | async-start | bytes 5242880 | tf_op jit(solution)/shard_map/all_gather | solution.py:47
  147.7 4.7 %copy-start.2 = (bf16[512]{0:T(512)(128)(2,1)S(1)}, bf16[512]{0:T(512)(128)(2,1)}, u32[]{:S(2)}) copy-start(bf16[512]{0:T(512)(128)(2,1)} %param.9) | copy-start | bytes 3076
  147.7 52.4 %all-to-all-start = ((bf16[512,4,512]{0,2,1:T(8,128)(2,1)}), bf16[512,4,512]{0,2,1:T(8,128)(2,1)}, u32[]{:S(2)}, u32[]{:S(2)}) async-start(bf16[512,4,512]{0,2,1:T(8,128)(2,1)} %bitcast.12), calls=%async_computation | async-start | bytes 4194304 | tf_op jit(solution)/shard_map/all_to_all | solution.py:42
  152.3 108.3 %reduce-scatter.3.cloned.1.call-start = ((), (), s32[]{:S(2)}) async-start(), calls=%async_computation.8 | async-start | bytes 5242880 | tf_op jit(solution)/shard_map/reduce_scatter | solution.py:56
  204.3 3.2 %copy-start = (bf16[512,4,512]{0,2,1:T(8,128)(2,1)S(1)}, bf16[512,4,512]{0,2,1:T(8,128)(2,1)}, u32[]{:S(2)}) copy-start(bf16[512,4,512]{0,2,1:T(8,128)(2,1)} %copy.12) | copy-start | bytes 6291460
  217.0 73.1 %copy-start.1 = (bf16[256,512]{1,0:T(8,128)(2,1)S(1)}, bf16[256,512]{1,0:T(8,128)(2,1)}, u32[]{:S(2)}) copy-start(bf16[256,512]{1,0:T(8,128)(2,1)} %fusion.9) | copy-start | bytes 786436
  217.0 73.1 %reduce-scatter.5.cloned.1.call-start = ((), (), s32[]{:S(2)}) async-start(), calls=%async_computation.9 | async-start | bytes 1310720 | tf_op jit(solution)/shard_map/reduce_scatter | solution.py:57
Sparse Core Ops, SparseCore 0:
  8.9 19.4 all-gather.5
  29.9 45.6 all-gather.7
  79.1 44.6 all-gather.9
  125.2 47.2 all-gather.11
  217.1 43.4 reduce-scatter.2
  262.7 27.2 reduce-scatter.4
where the time goes:
time: 299 us
  waiting for transfers between devices  243 us (81%)
  between operations  13.5 us (5%)
  matrix products  12.7 us (4%)
  local copies, waits for them, and re-layouts  10.6 us (4%)
  starting transfers between devices  8.42 us (3%)
  blocking collectives  5.37 us (2%)
  other arithmetic  4.95 us (2%)
    all_gather x1, waiting for transfers between devices, spread_body(): out_full = lax.all_gather(out_weight, 'fs', axis=0, tiled=True)  47.3 us
    reduce_scatter x1, waiting for transfers between devices, spread_body(): columns = lax.psum_scatter(partials, 'tp', scatter_dimension=1, tiled=True)  43.6 us
    all_gather x1, waiting for transfers between devices, spread_body(): rows = lax.all_gather(resid, 'fs', axis=0, tiled=True)  41.1 us
    all_to_all x1, waiting for transfers between devices, spread_body(): lax.all_to_all(up_weight, 'fs', split_axis=1, concat_axis=0, tiled=True)  40 us
    reduce_scatter x1, waiting for transfers between devices, spread_body(): branch = lax.psum_scatter(columns, 'fs', scatter_dimension=0, tiled=True)  29.4 us
    all_gather x1, waiting for transfers between devices, spread_body(): mixed_whole = lax.all_gather(mixed, 'tp', axis=1, tiled=True)  20.3 us
    all_to_all x1, waiting for transfers between devices, spread_body(): lax.all_to_all(down_weight, 'fs', split_axis=0, concat_axis=1, tiled=True)  20 us
    dot_general x1, matrix products, spread_body(): jnp.dot(activated, down_mine, preferred_element_type=jnp.float32)  9.4 us
  transfers between devices with their start and end apart: 8, of which 7 were waited for; matrix products, arithmetic and copies ran while one was open for 4% of the time, Pallas kernels for 0%

commit v1 on v0

--- a/solution.py
+++ b/solution.py
@@ -37,7 +37,12 @@
 
 
 def spread_body(stream, mixed, out_weight, norm_gain, up_weight, down_weight):
-    mixed_whole = lax.all_gather(mixed, "tp", axis=1, tiled=True)
+    ring = [mixed]
+    for hop in range(3):
+        ring.append(lax.ppermute(ring[-1], "tp", [(dev, (dev + 1) % 4) for dev in range(4)]))
+    mixed_whole = jnp.roll(
+        jnp.concatenate(ring[::-1], axis=1), (lax.axis_index("tp") + 1) * ring[0].shape[1], axis=1
+    )
     out_full = lax.all_gather(out_weight, "fs", axis=0, tiled=True)
     up_mine = lax.all_to_all(up_weight, "fs", split_axis=1, concat_axis=0, tiled=True)
     down_mine = lax.all_to_all(down_weight, "fs", split_axis=0, concat_axis=1, tiled=True)

time: 299 us -> 280 us (0.936)
  waiting for transfers between devices: 243 us -> 224 us
    all_gather x1 -> x0, waiting for transfers between devices: 20.3 us -> none  [spread_body(): mixed_whole = lax.all_gather(mixed, 'tp', axis=1, tiled=True)]
    ppermute x0 -> x3, waiting for transfers between devices: none -> 17.8 us  [spread_body(): lax.ppermute(ring[-1], 'tp', [(dev, (dev + 1) % 4) for dev in range(4)])]
    all_gather x1, waiting for transfers between devices: 47.3 us -> 31.4 us  [spread_body(): out_full = lax.all_gather(out_weight, 'fs', axis=0, tiled=True)]
  transfers between devices with their start and end apart: 8 -> 10, of which waited for: 7 -> 9; matrix products, arithmetic and copies ran while one was open for 4% -> 4% of each run, Pallas kernels for 0% -> 0%
where the time goes in v1:
time: 280 us
  waiting for transfers between devices  224 us (80%)
  between operations  13.3 us (5%)
  matrix products  12.4 us (4%)
  local copies, waits for them, and re-layouts  10.8 us (4%)
  starting transfers between devices  8.96 us (3%)
  blocking collectives  5.36 us (2%)
  other arithmetic  4.95 us (2%)
    reduce_scatter x1, waiting for transfers between devices, spread_body(): columns = lax.psum_scatter(partials, 'tp', scatter_dimension=1, tiled=True)  43.5 us
    all_gather x1, waiting for transfers between devices, spread_body(): rows = lax.all_gather(resid, 'fs', axis=0, tiled=True)  41.1 us
    all_to_all x1, waiting for transfers between devices, spread_body(): lax.all_to_all(up_weight, 'fs', split_axis=1, concat_axis=0, tiled=True)  40 us
    all_gather x1, waiting for transfers between devices, spread_body(): out_full = lax.all_gather(out_weight, 'fs', axis=0, tiled=True)  31.4 us
    reduce_scatter x1, waiting for transfers between devices, spread_body(): branch = lax.psum_scatter(columns, 'fs', scatter_dimension=0, tiled=True)  29.4 us
    all_to_all x1, waiting for transfers between devices, spread_body(): lax.all_to_all(down_weight, 'fs', split_axis=0, concat_axis=1, tiled=True)  20 us
    ppermute x3, waiting for transfers between devices, spread_body(): lax.ppermute(ring[-1], 'tp', [(dev, (dev + 1) % 4) for dev in range(4)])  17.8 us
    dot_general x1, matrix products, spread_body(): jnp.dot(activated, down_mine, preferred_element_type=jnp.float32)  9.41 us
  transfers between devices with their start and end apart: 10, of which 9 were waited for; matrix products, arithmetic and copies ran while one was open for 4% of the time, Pallas kernels for 0%

profile of v1, /device:TPU:0, one launch (start us, length us, event | category | flops | bytes accessed | tf_op | source)
XLA Modules:
  0.0 279.7 jit_solution(2316502643768820807)
XLA Ops:
  6.5 0.7 all-gather.5.cloned.1.call-update
  7.3 0.5 collective-permute-start
  7.8 6.2 %collective-permute-done = bf16[256,512]{1,0:T(8,128)(2,1)S(1)} collective-permute-done((bf16[256,512]{1,0:T(8,128)(2,1)}, bf16[256,512]{1,0:T(8,128)(2,1)S(1)}, u32[]{:S(2)}, u32[]{:S(2)}) %collective-permute-start) | collective-permute-done | bytes 262176 | tf_op jit(solution)/shard_map/ppermute | solution.py:42
  14.1 0.0 collective-permute-start.1
  14.1 5.8 %collective-permute-done.1 = bf16[256,512]{1,0:T(8,128)(2,1)S(1)} collective-permute-done((bf16[256,512]{1,0:T(8,128)(2,1)S(1)}, bf16[256,512]{1,0:T(8,128)(2,1)S(1)}, u32[]{:S(2)}, u32[]{:S(2)}) %collective-permute-start.1) | collective-permute-done | bytes 262176 | tf_op jit(solution)/shard_map/ppermute | solution.py:42
  19.9 5.8 %collective-permute-done.2 = bf16[256,512]{1,0:T(8,128)(2,1)S(1)} collective-permute-done((bf16[256,512]{1,0:T(8,128)(2,1)S(1)}, bf16[256,512]{1,0:T(8,128)(2,1)S(1)}, u32[]{:S(2)}, u32[]{:S(2)}) %collective-permute-start.2) | collective-permute-done | bytes 262176 | tf_op jit(solution)/shard_map/ppermute | solution.py:42
  25.9 31.4 %all-gather.5.cloned.1.call-done = bf16[2048,512]{1,0:T(8,128)(2,1)} async-done(((bf16[512,512]{1,0:T(8,128)(2,1)}), bf16[2048,512]{1,0:T(8,128)(2,1)}) %all-gather.5.cloned.1.call-update) | async-done | bytes 2097168 | tf_op jit(solution)/shard_map/all_gather | solution.py:46
  57.3 3.0 %fusion.9 = bf16[256,512]{1,0:T(8,128)(2,1)} fusion(bf16[2048,512]{1,0:T(8,128)(2,1)} %all-gather.5.cloned.1.call-done, bf16[256,4096]{1,0:T(8,128)(2,1)S(1)} %constant_dynamic-update-slice_fusion, s32[]{:T(128)S(6)} %select_n.14, bf16[256,512]{1,0:T(8,128)(2,1)S(1)} %copy-done.4), kind=kOutput, calls=%fused_computation.11 | convolution fusion | flops 537264128 | bytes 3670020 | tf_op jit(solution)/shard_map/dot_general | solution.py:49
  60.3 3.6 %all-to-all-start.1 = ((bf16[4,512,512]{2,1,0:T(8,128)(2,1)}), bf16[4,512,512]{2,1,0:T(8,128)(2,1)S(1)}, u32[]{:S(2)}, u32[]{:S(2)}) async-start(bf16[4,512,512]{2,1,0:T(8,128)(2,1)} %bitcast.12), calls=%async_computation.1 | async-start | bytes 4194304 | tf_op jit(solution)/shard_map/all_to_all | solution.py:48
  64.0 41.1 %all-gather.7.cloned.1.call-done = bf16[1024,512]{1,0:T(8,128)(2,1)} async-done(((bf16[256,512]{1,0:T(8,128)(2,1)}), bf16[1024,512]{1,0:T(8,128)(2,1)}) %all-gather.7.cloned.1.call-update) | async-done | bytes 1048592 | tf_op jit(solution)/shard_map/all_gather | solution.py:51
  105.2 3.9 %copy.10 = bf16[512,2048]{0,1:T(8,128)(2,1)} copy(bf16[512,2048]{1,0:T(8,128)(2,1)} %param.10) | data formatting | bytes 4194304 | tf_op args[4]
  109.1 20.0 %all-to-all-done.1 = bf16[4,512,512]{2,1,0:T(8,128)(2,1)S(1)} async-done(((bf16[4,512,512]{2,1,0:T(8,128)(2,1)}), bf16[4,512,512]{2,1,0:T(8,128)(2,1)S(1)}, u32[]{:S(2)}, u32[]{:S(2)}) %all-to-all-start.1) | async-done | bytes 2097184 | tf_op jit(solution)/shard_map/all_to_all | solution.py:48
  129.1 4.6 %all-to-all-start = ((bf16[512,4,512]{0,2,1:T(8,128)(2,1)}), bf16[512,4,512]{0,2,1:T(8,128)(2,1)}, u32[]{:S(2)}, u32[]{:S(2)}) async-start(bf16[512,4,512]{0,2,1:T(8,128)(2,1)} %bitcast.11), calls=%async_computation | async-start | bytes 4194304 | tf_op jit(solution)/shard_map/all_to_all | solution.py:47
  133.7 0.0 reduce-scatter.3.cloned.1.call-start
  133.8 5.4 %all-gather = bf16[4,1,512]{2,1,0:T(2,128)(2,1)S(1)} all-gather(bf16[1,1,512]{2,1,0:T(2,128)(2,1)S(1)} %reshape.15), channel_id=1, replica_groups=mesh['grp'=2,'fs'=4,'tp'=4] {'tp'}, dimensions={0}, use_global_device_ids=true | all-gather | bytes 5120 | tf_op jit(solution)/shard_map/all_gather | solution.py:53
  139.1 2.4 copy.12
  141.5 40.0 %all-to-all-done = bf16[512,4,512]{0,2,1:T(8,128)(2,1)} async-done(((bf16[512,4,512]{0,2,1:T(8,128)(2,1)}), bf16[512,4,512]{0,2,1:T(8,128)(2,1)}, u32[]{:S(2)}, u32[]{:S(2)}) %all-to-all-start) | async-done | bytes 2097184 | tf_op jit(solution)/shard_map/all_to_all | solution.py:47
  181.5 4.2 %copy.11 = bf16[4,512,512]{2,1,0:T(8,128)(2,1)} copy(bf16[4,512,512]{1,2,0:T(8,128)(2,1)} %bitcast.2) | data formatting | bytes 4194304 | tf_op jit(solution)/shard_map/all_to_all | solution.py:47
  185.7 3.2 %fusion = f32[1024]{0:T(1024)S(1)} fusion(bf16[1024,2048]{1,0:T(8,128)(2,1)} %all-gather.9.cloned.1.call-done), kind=kLoop, calls=%fused_computation.2 | loop fusion | flops 6290432 | bytes 4198400 | tf_op jit(solution)/shard_map/reduce_sum | solution.py:54
  189.0 9.4 %convolution_convert_fusion = bf16[1024,2048]{1,0:T(8,128)(2,1)} fusion(bf16[512,2048]{0,1:T(8,128)(2,1)S(1)} %bitcast.13, bf16[2048,512]{1,0:T(8,128)(2,1)} %bitcast.14, bf16[1024,2048]{1,0:T(8,128)(2,1)} %all-gather.9.cloned.1.call-done, f32[2048]{0:T(1024)S(1)} %bitcast.15, f32[1024]{0:T(1024)S(1)} %add_rsqrt_fusion), kind=kOutput, calls=%fused_computation.8 | convolution fusion | flops 4307025920 | bytes 12595200 | tf_op jit(solution)/shard_map/dot_general | solution.py:58
  198.4 0.0 reduce-scatter.5.cloned.1.call-start
  198.4 43.5 %reduce-scatter.3.cloned.1.call-done = bf16[1024,512]{1,0:T(8,128)(2,1)} async-done(((bf16[1024,2048]{1,0:T(8,128)(2,1)}), bf16[1024,512]{1,0:T(8,128)(2,1)}) %reduce-scatter.3.cloned.1.call-update) | async-done | bytes 1048592 | tf_op jit(solution)/shard_map/reduce_scatter | solution.py:61
  242.0 29.4 %reduce-scatter.5.cloned.1.call-done = bf16[256,512]{1,0:T(8,128)(2,1)} async-done(((bf16[1024,512]{1,0:T(8,128)(2,1)}), bf16[256,512]{1,0:T(8,128)(2,1)}) %reduce-scatter.5.cloned.1.call-update) | async-done | bytes 262160 | tf_op jit(solution)/shard_map/reduce_scatter | solution.py:62
  271.4 1.7 add_convert_fusion
  (30 shorter events, 0.4 us)
Async XLA Ops:
  6.5 19.2 %copy-start.2 = (bf16[256,512]{1,0:T(8,128)(2,1)S(1)}, bf16[256,512]{1,0:T(8,128)(2,1)}, u32[]{:S(2)}) copy-start(bf16[256,512]{1,0:T(8,128)(2,1)} %param.7) | copy-start | bytes 786436
  6.5 50.8 %all-gather.5.cloned.1.call-start = ((), (), s32[]{:S(2)}) async-start(), calls=%async_computation.4 | async-start | bytes 2621440 | tf_op jit(solution)/shard_map/all_gather | solution.py:46
  7.3 97.9 %all-gather.7.cloned.1.call-start = ((), (), s32[]{:S(2)}) async-start(), calls=%async_computation.5 | async-start | bytes 1310720 | tf_op jit(solution)/shard_map/all_gather | solution.py:51
  7.3 6.8 %collective-permute-start = (bf16[256,512]{1,0:T(8,128)(2,1)}, bf16[256,512]{1,0:T(8,128)(2,1)S(1)}, u32[]{:S(2)}, u32[]{:S(2)}) collective-permute-start(bf16[256,512]{1,0:T(8,128)(2,1)} %param.7), channel_id=1, source_target_pairs={{0,1},{1,2},{2,3},{3,0},{4,5},{5,6},{6,7},{7,4},{8,9},{9,10},{10,1... | collective-permute-start | bytes 786440 | tf_op jit(solution)/shard_map/ppermute | solution.py:42
  14.1 5.8 %collective-permute-start.1 = (bf16[256,512]{1,0:T(8,128)(2,1)S(1)}, bf16[256,512]{1,0:T(8,128)(2,1)S(1)}, u32[]{:S(2)}, u32[]{:S(2)}) collective-permute-start(bf16[256,512]{1,0:T(8,128)(2,1)S(1)} %collective-permute-done), channel_id=1, source_target_pairs={{0,1},{1,2},{2,3},{3,0},{4,5},{5,6},{6,7},{7,4},{8,9},{9,10},{10,1... | collective-permute-start | bytes 786440 | tf_op jit(solution)/shard_map/ppermute | solution.py:42
  19.9 5.8 %collective-permute-start.2 = (bf16[256,512]{1,0:T(8,128)(2,1)S(1)}, bf16[256,512]{1,0:T(8,128)(2,1)S(1)}, u32[]{:S(2)}, u32[]{:S(2)}) collective-permute-start(bf16[256,512]{1,0:T(8,128)(2,1)S(1)} %collective-permute-done.1), channel_id=1, source_target_pairs={{0,1},{1,2},{2,3},{3,0},{4,5},{5,6},{6,7},{7,4},{8,9},{9,10},{10,1... | collective-permute-start | bytes 786440 | tf_op jit(solution)/shard_map/ppermute | solution.py:42
  19.9 37.5 %copy-start.4 = (bf16[256,512]{1,0:T(8,128)(2,1)S(1)}, bf16[256,512]{1,0:T(8,128)(2,1)}, u32[]{:S(2)}) copy-start(bf16[256,512]{1,0:T(8,128)(2,1)} %param.6) | copy-start | bytes 786436
  60.3 68.8 %all-to-all-start.1 = ((bf16[4,512,512]{2,1,0:T(8,128)(2,1)}), bf16[4,512,512]{2,1,0:T(8,128)(2,1)S(1)}, u32[]{:S(2)}, u32[]{:S(2)}) async-start(bf16[4,512,512]{2,1,0:T(8,128)(2,1)} %bitcast.12), calls=%async_computation.1 | async-start | bytes 4194304 | tf_op jit(solution)/shard_map/all_to_all | solution.py:48
  64.0 121.7 %all-gather.9.cloned.1.call-start = ((), (), s32[]{:S(2)}) async-start(), calls=%async_computation.6 | async-start | bytes 5242880 | tf_op jit(solution)/shard_map/all_gather | solution.py:52
  129.1 4.6 %copy-start.3 = (bf16[512]{0:T(512)(128)(2,1)S(1)}, bf16[512]{0:T(512)(128)(2,1)}, u32[]{:S(2)}) copy-start(bf16[512]{0:T(512)(128)(2,1)} %param.9) | copy-start | bytes 3076
  129.1 52.4 %all-to-all-start = ((bf16[512,4,512]{0,2,1:T(8,128)(2,1)}), bf16[512,4,512]{0,2,1:T(8,128)(2,1)}, u32[]{:S(2)}, u32[]{:S(2)}) async-start(bf16[512,4,512]{0,2,1:T(8,128)(2,1)} %bitcast.11), calls=%async_computation | async-start | bytes 4194304 | tf_op jit(solution)/shard_map/all_to_all | solution.py:47
  133.7 108.3 %reduce-scatter.3.cloned.1.call-start = ((), (), s32[]{:S(2)}) async-start(), calls=%async_computation.7 | async-start | bytes 5242880 | tf_op jit(solution)/shard_map/reduce_scatter | solution.py:61
  185.7 3.2 %copy-start = (bf16[512,4,512]{0,2,1:T(8,128)(2,1)S(1)}, bf16[512,4,512]{0,2,1:T(8,128)(2,1)}, u32[]{:S(2)}) copy-start(bf16[512,4,512]{0,2,1:T(8,128)(2,1)} %copy.12) | copy-start | bytes 6291460
  198.4 73.1 %copy-start.1 = (bf16[256,512]{1,0:T(8,128)(2,1)S(1)}, bf16[256,512]{1,0:T(8,128)(2,1)}, u32[]{:S(2)}) copy-start(bf16[256,512]{1,0:T(8,128)(2,1)} %fusion.9) | copy-start | bytes 786436
  198.4 73.0 %reduce-scatter.5.cloned.1.call-start = ((), (), s32[]{:S(2)}) async-start(), calls=%async_computation.8 | async-start | bytes 1310720 | tf_op jit(solution)/shard_map/reduce_scatter | solution.py:62
Sparse Core Ops, SparseCore 0:
  8.9 48.3 all-gather.4
  60.5 44.6 all-gather.6
  106.7 47.2 all-gather.8
  198.5 43.4 reduce-scatter.2
  244.1 27.2 reduce-scatter.4
